TPU v7x, 32 devices: a whole 2x2x4 slice. The times are simulated.
32 devices in a mesh: grp: 2 (over y), sp: 4 (over z), tp: 4 (over x, core).
Axes of the slice: x: 2, y: 2, z: 4, core: 2. Of those that a mesh axis runs over, the one named last changes fastest.
Arguments:
- query_rows: bfloat16 [1024, 1024], P(('grp', 'sp'), 'tp'), parts along dimension 0, may hold values from -64 to 64
- key_rows: bfloat16 [1024, 512], P(('grp', 'sp'), 'tp'), parts along dimension 0, may hold values from -16 to 16
- value_rows: bfloat16 [1024, 512], P(('grp', 'sp'), 'tp'), parts along dimension 0, may hold values from -6 to 6
- sink_logit: float32 [16], P('tp'), may hold values from 3.5 to 7
- out_weight: bfloat16 [1024, 2048], P('tp'), may hold values from -0.1875 to 0.1875
- residual: bfloat16 [1024, 2048], P(('grp', 'sp', 'tp')), parts along dimension 0, may hold values from -6 to 6
- norm_gain: float32 [2048], replicated, may hold values from 0.1 to 1.9
- routes: int32 [1024, 6], P(('grp', 'sp', 'tp')), parts along dimension 0, may hold values from 0 to 15, as said below
- gate_weights: float32 [1024, 6], P(('grp', 'sp', 'tp')), parts along dimension 0, may hold values from 0.1 to 0.8
- expert_gate: bfloat16 [16, 2048, 512], P(('sp', 'tp')), may hold values from -0.125 to 0.125
- expert_up: bfloat16 [16, 2048, 512], P(('sp', 'tp')), may hold values from -0.125 to 0.125
- expert_down: bfloat16 [16, 512, 2048], P(('sp', 'tp')), may hold values from -0.25 to 0.25
- shared_gate: bfloat16 [2048, 512], P(None, 'tp'), may hold values from -0.125 to 0.125
- shared_up: bfloat16 [2048, 512], P(None, 'tp'), may hold values from -0.125 to 0.125
- shared_down: bfloat16 [512, 2048], P('tp'), may hold values from -0.25 to 0.25
Outputs:
- layer_out: bfloat16 [1024, 2048], P(('grp', 'sp', 'tp')), parts along dimension 0
There are 2 independent parts, one for each index of `grp`. A program takes and returns all parts, laid end to end along the dimension named above; an argument that names none is the same for every part. Nothing has to cross between parts.
Inputs may be any that keep to these rules, and one draw needn't show every extreme that they name: `routes`: in each aligned block of 32 rows (the rows of one device) every row names 6 different experts and no expert is named by more than 24 rows; in every draw some expert is named by exactly 24 rows of every block.
All inputs are finite; a program needn't handle non-finite values.
Results may differ from a plain program's by a relative error of at most 0.015.
Values may be sent and summed in bfloat16 or wider, within the bound.
No kernel may reach another device: no remote copies, remote signals or barrier semaphores. Data moves between devices by JAX's collectives and lax.ppermute only.
A program may use at most 64 MiB of HBM per device.

v0:
```python
import functools

import jax
import jax.numpy as jnp
from jax import lax
from jax.experimental import pallas as pl
from jax.experimental.pallas import tpu as pltpu
from jax.sharding import PartitionSpec as P

HEAD = 64
WINDOW = 128
TOPK = 6
LANES = 128
SLAB_WORK = 1 << 30
FILL_WORK = 1 << 31
VMEM_BYTES = 12 * 1024 * 1024

norm_eps = 1e-06


def with_halo(block, sides, width):
    for axis, dim in sides:
        count = lax.axis_size(axis)
        forward = [(i, i + 1) for i in range(count - 1)]
        backward = [(target, source) for source, target in forward]
        low = lax.ppermute(
            lax.slice_in_dim(block, block.shape[dim] - width, None, axis=dim), axis, forward
        )
        high = lax.ppermute(lax.slice_in_dim(block, 0, width, axis=dim), axis, backward)
        block = jnp.concatenate([low, block, high], axis=dim)
    return block


def window_attention(query_rows, key_rows, value_rows, sink_logit):
    local_len = query_rows.shape[0]
    head_size = HEAD
    local_kv = key_rows.shape[1] // head_size
    local_heads = query_rows.shape[1] // head_size
    grouped = local_heads // local_kv
    blocks = local_len // WINDOW
    stacked = jnp.stack([key_rows, value_rows])
    widened = with_halo(stacked, (("sp", 1),), WINDOW)
    banded = widened.reshape(2, blocks + 2, WINDOW, local_kv, head_size)
    banded = jnp.concatenate([banded[:, :-2], banded[:, 1:-1], banded[:, 2:]], axis=2)
    queries = query_rows.reshape(blocks, WINDOW, local_kv, grouped, head_size)
    scores = jnp.einsum(
        "nqhgd,nkhd->nhgqk", queries, banded[0], preferred_element_type=jnp.float32
    ) * head_size ** (-0.5)
    seq_start = lax.axis_index("sp") * local_len
    total_len = lax.axis_size("sp") * local_len
    block_ids = jnp.arange(blocks, dtype=jnp.int32)[:, None, None]
    query_pos = seq_start + block_ids * WINDOW + jnp.arange(WINDOW, dtype=jnp.int32)[None, :, None]
    key_pos = (
        seq_start
        + (block_ids - 1) * WINDOW
        + jnp.arange(3 * WINDOW, dtype=jnp.int32)[None, None, :]
    )
    in_window = (jnp.abs(key_pos - query_pos) <= WINDOW) & (key_pos >= 0) & (key_pos < total_len)
    scores = jnp.where(in_window[:, None, None], scores, -jnp.inf)
    sink_part = sink_logit.reshape(1, local_kv, grouped, 1, 1)
    row_max = jnp.maximum(sink_part, jnp.max(scores, axis=-1, keepdims=True))
    shifted = jnp.exp(scores - row_max)
    denominator = jnp.exp(sink_part - row_max) + jnp.sum(shifted, axis=-1, keepdims=True)
    weights = (shifted / denominator).astype(jnp.bfloat16)
    attended = jnp.einsum(
        "nhgqk,nkhd->nqhgd", weights, banded[1], preferred_element_type=jnp.float32
    )
    return attended.astype(jnp.bfloat16).reshape(local_len, local_heads * head_size)


def rms_norm(stream, norm_gain):
    return (
        stream * lax.rsqrt(jnp.mean(stream * stream, axis=-1, keepdims=True) + norm_eps) * norm_gain
    ).astype(jnp.bfloat16)


def gated(rows, gate, up):
    gate_part = jnp.dot(rows, gate, preferred_element_type=jnp.float32)
    up_part = jnp.dot(rows, up, preferred_element_type=jnp.float32)
    return (jax.nn.silu(gate_part) * up_part).astype(jnp.bfloat16)


def dispatched_layer(attended, operands):
    out_weight, residual, norm_gain, routes, gate_weights = operands[:5]
    expert_gate, expert_up, expert_down, shared_gate, shared_up, shared_down = operands[5:]
    tok_dev = attended.shape[0]
    tok_rows = residual.shape[0]
    model_width = residual.shape[1]
    projected = lax.psum_scatter(
        jnp.dot(attended, out_weight, preferred_element_type=jnp.float32).astype(jnp.bfloat16),
        "tp",
        scatter_dimension=0,
        tiled=True,
    ).astype(jnp.float32)
    stream = residual.astype(jnp.float32) + projected
    normed = rms_norm(stream, norm_gain)
    sp_count = lax.axis_size("sp")
    tp_count = lax.axis_size("tp")
    experts_all = sp_count * tp_count
    capacity = (2 * tok_dev * TOPK + tp_count * experts_all - 1) // (tp_count * experts_all)
    copies = tok_rows * TOPK
    flat_expert = routes.reshape(-1)
    one_hot = (flat_expert[:, None] == jnp.arange(experts_all, dtype=jnp.int32)[None, :]).astype(
        jnp.int32
    )
    rank_in_expert = jnp.sum(jnp.cumsum(one_hot, axis=0) * one_hot, axis=1) - 1
    target_slot = flat_expert * capacity + rank_in_expert
    slot_token = (
        jnp.full((experts_all * capacity,), tok_rows, jnp.int32)
        .at[target_slot]
        .set(jnp.arange(copies, dtype=jnp.int32) // TOPK)
    )
    padded_rows = jnp.concatenate([normed, jnp.zeros((1, model_width), jnp.bfloat16)], axis=0)
    outgoing = padded_rows[slot_token].reshape(experts_all, capacity, model_width)
    incoming = lax.all_to_all(outgoing, ("sp", "tp"), split_axis=0, concat_axis=0, tiled=True)
    hidden = gated(incoming.reshape(-1, model_width), expert_gate[0], expert_up[0])
    result = jnp.dot(hidden, expert_down[0], preferred_element_type=jnp.float32).astype(
        jnp.bfloat16
    )
    returned = lax.all_to_all(
        result.reshape(incoming.shape), ("sp", "tp"), split_axis=0, concat_axis=0, tiled=True
    )
    returned = returned.reshape(experts_all * capacity, model_width)
    gathered_copies = returned[target_slot].reshape(tok_rows, TOPK, model_width)
    routed = jnp.sum(gate_weights[:, :, None] * gathered_copies.astype(jnp.float32), axis=1)
    slab_rows = lax.all_gather(normed, "tp", axis=0, tiled=True)
    hidden = gated(slab_rows, shared_gate, shared_up)
    partials = jnp.dot(hidden, shared_down, preferred_element_type=jnp.float32)
    shared = lax.psum_scatter(
        partials.astype(jnp.bfloat16), "tp", scatter_dimension=0, tiled=True
    ).astype(jnp.float32)
    return (stream + routed + shared).astype(jnp.bfloat16)


def dot32(left, right):
    return jnp.dot(left, right, preferred_element_type=jnp.float32)


def later(index):
    return ((index + 1) ^ 1) - 1


def fill_kernel(given, sources, results, arrival):
    for copy in fetch(sources, results, arrival):
        copy.wait()


def pack_kernel(given, sources, results, arrival):
    rows = sources[0].shape[0]
    halves = [results[0].at[pl.ds(index * rows, rows)] for index in range(2)]
    fill_kernel(given, sources, halves, arrival)


def attention_kernel(total_len, given, sources, results, arrival):
    place_ref, sink_ref, query_ref, pack_ref, weight_ref = given
    kept_ref, sent_ref, attended_ref, *packs = results
    packs = [pack_ref, *packs]
    rows = query_ref.shape[0]
    copies = fetch(sources, packs[1:], arrival)
    heads = query_ref.shape[1] // HEAD
    kv_heads = pack_ref.shape[1] // HEAD
    grouped = heads // kv_heads
    here, me = place_ref[0], place_ref[1]
    span = (grouped * rows, 3 * rows)
    row = lax.broadcasted_iota(jnp.int32, span, 0)
    col = lax.broadcasted_iota(jnp.int32, span, 1)
    first = jnp.where(col < 2 * rows, ((here ^ 1) - 1) * rows, (later(here) - 2) * rows)
    key_pos = col + jnp.where(col < rows, here * rows, first)
    query_pos = here * rows + row % rows
    near = (jnp.abs(key_pos - query_pos) <= WINDOW) & (key_pos >= 0) & (key_pos < total_len)
    head_of = row[:, :1] // rows
    for copy in copies:
        copy.wait()
    keys = jnp.concatenate([pack[:rows] for pack in packs], axis=0)
    values = jnp.concatenate([pack[rows:] for pack in packs], axis=0)
    for group in range(kv_heads):
        lanes = slice(group * HEAD, (group + 1) * HEAD)
        first_head = group * grouped
        queries = jnp.concatenate(
            [
                query_ref[:, head * HEAD : (head + 1) * HEAD]
                for head in range(first_head, first_head + grouped)
            ],
            axis=0,
        )
        scores = lax.dot_general(
            queries, keys[:, lanes], (((1,), (1,)), ((), ())), preferred_element_type=jnp.float32
        )
        scores = jnp.where(near, scores * HEAD ** (-0.5), -jnp.inf)
        sink = jnp.full(head_of.shape, sink_ref[first_head], jnp.float32)
        for offset in range(1, grouped):
            sink = jnp.where(head_of == offset, sink_ref[first_head + offset], sink)
        row_max = jnp.maximum(sink, jnp.max(scores, axis=1, keepdims=True))
        shifted = jnp.exp(scores - row_max)
        denominator = jnp.exp(sink - row_max) + jnp.sum(shifted, axis=1, keepdims=True)
        weights = (shifted / denominator).astype(jnp.bfloat16)
        out = dot32(weights, values[:, lanes]).astype(jnp.bfloat16)
        for offset in range(grouped):
            head = first_head + offset
            attended_ref[:, head * HEAD : (head + 1) * HEAD] = out[offset * rows : (offset + 1) * rows]
    count = kept_ref.shape[0] // 2

    def block_of(peer):
        start = pl.multiple_of((me ^ peer) * count, count)
        return attended_ref[pl.ds(start, count), :]

    def project(one, other):
        return dot32(jnp.concatenate([block_of(one), block_of(other)], axis=0), weight_ref[...])

    sent_ref[...] = project(1, 3).astype(jnp.bfloat16)
    kept_ref[...] = project(0, 2)


def norm_kernel(experts_all, given, sources, results, arrival):
    stream_ref, payload_ref = results[:2]
    for copy in fetch(sources, results[2:], arrival):
        copy.wait()
    residual = given[0]
    kept, sibling, peer, gain, routes, gates = results[2:]
    rows, width = residual.shape
    stream = residual[...].astype(jnp.float32) + kept[:rows]
    stream = stream + sibling[:rows].astype(jnp.float32) + peer[...].astype(jnp.float32)
    stream_ref[...] = stream
    scale = lax.rsqrt(jnp.mean(stream * stream, axis=1, keepdims=True) + norm_eps)
    payload_ref[:, :width] = (stream * scale * gain[...]).astype(jnp.bfloat16)
    shape = (payload_ref.shape[1] - width, rows)
    lane = lax.broadcasted_iota(jnp.int32, shape, 0)
    expert = jnp.where(lane < experts_all, lane, lane - experts_all)
    dense = jnp.zeros(shape, jnp.float32)
    for copy in range(routes.shape[0]):
        chosen = routes[copy : copy + 1] == expert
        dense = dense + jnp.where(chosen, gates[copy : copy + 1], 0.0)
    high = dense.astype(jnp.bfloat16).astype(jnp.float32)
    spread = jnp.where(lane < experts_all, high, dense - high)
    payload_ref[:, width:] = spread.T.astype(jnp.bfloat16)


def slab_kernel(experts_all, given, sources, results, arrival):
    outs, refs = results[:4], results[4:]
    count = sources[0].shape[0]
    expert_ref, slab_ref = given[0], refs[-1]
    weights = given[1:] if len(given) > 1 else refs[:3]
    shared = refs[3:-1]
    pieces = [slab_ref.at[pl.ds(index * count, count)] for index in range(4)]
    copies = fetch(sources, [*pieces, *refs[:-1]], arrival)
    for copy in copies[:4]:
        copy.wait()
    coming = copies[4:]
    width = outs[0].shape[1]
    rows = slab_ref[:, :width]
    tail = slab_ref[:, width:].astype(jnp.float32)
    lane = lax.broadcasted_iota(jnp.int32, tail.shape, 1)
    mine = (lane == expert_ref[0]) | (lane == expert_ref[0] + experts_all)
    weight = jnp.sum(jnp.where(mine, tail, 0.0), axis=1, keepdims=True)

    def arrived(ref):
        if coming:
            coming.pop(0).wait()
        return ref[...]

    def ffn(gate, up, down):
        gate_part = dot32(rows, arrived(gate))
        up_part = dot32(rows, arrived(up))
        hidden = (gate_part / (1.0 + jnp.exp(-gate_part)) * up_part).astype(jnp.bfloat16)
        return dot32(hidden, arrived(down)).astype(jnp.bfloat16).astype(jnp.float32)

    part = weight * ffn(*weights)
    if shared:
        part = part + ffn(*shared)
    for index, out in enumerate(outs):
        out[...] = part[index * count : (index + 1) * count].astype(out.dtype)


def on_core(kernel, work, outs, smem, placed, fetched, scratch=(), arguments=()):
    in_vmem = pl.BlockSpec(memory_space=pltpu.VMEM)
    fetched = [
        pltpu.with_memory_space_constraint(array, pltpu.HBM) if index in arguments else array
        for index, array in enumerate(fetched)
    ]
    inputs = len(smem) + len(placed) + len(fetched)
    first = inputs - len(fetched)

    def run(*refs):
        sources = refs[first:inputs]
        arrival = refs[-1]
        kernel(refs[: first], sources, refs[inputs:-1], arrival)

    return pl.pallas_call(
        run,
        out_shape=tuple(outs),
        in_specs=[pl.BlockSpec(memory_space=pltpu.SMEM)] * len(smem)
        + [in_vmem] * len(placed)
        + [pl.BlockSpec(memory_space=pl.ANY)] * len(fetched),
        out_specs=tuple(in_vmem for _ in outs),
        scratch_shapes=[*scratch, pltpu.SemaphoreType.DMA((len(fetched),))],
        compiler_params=pltpu.CompilerParams(vmem_limit_bytes=VMEM_BYTES),
        cost_estimate=pl.CostEstimate(flops=work, transcendentals=0, bytes_accessed=0),
    )(*smem, *placed, *fetched)


def fetch(sources, targets, arrival):
    copies = [
        pltpu.make_async_copy(source, target, arrival.at[index])
        for index, (source, target) in enumerate(zip(sources, targets))
    ]
    for copy in copies:
        copy.start()
    return copies


def room(array):
    return pltpu.VMEM(array.shape, array.dtype)


def flip(value, bit):
    count = lax.axis_size("tp")
    return lax.ppermute(value, "tp", [(i, i ^ bit) for i in range(count)])


def swap(value, bits):
    count = lax.axis_size("sp")
    return lax.ppermute(value, "sp", [(i, i ^ bits) for i in range(count)])


def neighbours(value):
    count = lax.axis_size("sp")
    even = [(i, i ^ 1) for i in range(count)]
    odd = [(i, later(i)) for i in range(1, count - 1)]
    from_even = lax.ppermute(value, "sp", even)
    return [from_even, lax.ppermute(value, "sp", odd)]


def gathered_layer(query_rows, key_rows, value_rows, sink_logit, operands):
    out_weight, residual, norm_gain, routes, gate_weights = operands[:5]
    expert_gate, expert_up, expert_down, shared_gate, shared_up, shared_down = operands[5:]
    count, width = residual.shape
    sp_count = lax.axis_size("sp")
    experts_all = sp_count * lax.axis_size("tp")
    here, me = lax.axis_index("sp"), lax.axis_index("tp")
    f32, bf16 = jnp.float32, jnp.bfloat16

    def held(rows, columns, dtype):
        return jax.ShapeDtypeStruct((rows, columns), dtype)

    local_len, kv_width = key_rows.shape
    [pack] = on_core(
        pack_kernel,
        0,
        [pltpu.VMEM((2 * local_len, kv_width), bf16)],
        [],
        [],
        [key_rows, value_rows],
        arguments=(0, 1),
    )
    wanted = [query_rows, out_weight, residual]
    query_here, out_here, residual_here = on_core(
        fill_kernel, SLAB_WORK, [room(array) for array in wanted], [], [], wanted,
        arguments=(0, 1, 2),
    )

    kept, sent = on_core(
        functools.partial(attention_kernel, sp_count * local_len),
        SLAB_WORK,
        [held(2 * count, width, f32), held(2 * count, width, bf16)],
        [
            jnp.stack([here, me]).astype(jnp.int32),
            pltpu.with_memory_space_constraint(sink_logit, pltpu.HBM),
        ],
        [query_here, pack, out_here],
        neighbours(pack),
        [room(query_rows)] + [pltpu.VMEM((2 * local_len, kv_width), bf16)] * 2,
    )
    sibling = flip(sent, 1)
    peer = flip((kept[count:] + sibling[count:].astype(f32)).astype(bf16), 2)
    tail = 2 * experts_all + -(2 * experts_all) % LANES
    terms = [kept, sibling, peer, norm_gain.reshape(1, width), routes.T, gate_weights.T]
    stream, payload = on_core(
        functools.partial(norm_kernel, experts_all),
        SLAB_WORK // 2,
        [held(count, width, f32), held(count, width + tail, bf16)],
        [],
        [residual_here],
        terms,
        [room(term) for term in terms],
        (3, 4, 5),
    )

    expert = (here * lax.axis_size("tp") + me).reshape(1).astype(jnp.int32)
    halves = [held(count, width, f32)] * 2 + [held(count, width, bf16)] * 2

    experts = [expert_gate[0], expert_up[0], expert_down[0]]
    shared = [shared_gate, shared_up, shared_down]
    slab_room = pltpu.VMEM((4 * count, width + tail), bf16)

    def pieces_of(rows):
        crossed = flip(rows, 2)
        return [rows, crossed, flip(rows, 1), flip(crossed, 1)]

    def returned(kept, kept_cross, sent, sent_cross):
        sent_cross = flip(sent_cross, 1)
        kept_cross = (kept_cross + sent_cross.astype(f32)).astype(bf16)
        sent = flip(sent, 1)
        return kept + sent.astype(f32) + flip(kept_cross, 2).astype(f32)

    kernel = functools.partial(slab_kernel, experts_all)
    *own, gate, up, down = on_core(
        kernel,
        FILL_WORK,
        halves + [room(array) for array in experts],
        [expert],
        [],
        [*pieces_of(payload), *experts, *shared],
        [*[room(array) for array in shared], slab_room],
        range(4, 10),
    )
    total = stream + returned(*own)
    for step in range(1, sp_count):
        parts = on_core(
            kernel,
            SLAB_WORK,
            halves,
            [expert],
            [gate, up, down],
            pieces_of(swap(payload, step)),
            [slab_room],
        )
        part = returned(*parts).astype(bf16)
        total = total + swap(part, step).astype(f32)
    return total.astype(bf16)


def body(query_rows, key_rows, value_rows, sink_logit, *operands):
    sp_count = lax.axis_size("sp")
    local_len = query_rows.shape[0]
    sent = 2 * operands[1].shape[0] * TOPK
    fits = lax.axis_size("tp") == 4 and sp_count & (sp_count - 1) == 0 and local_len == WINDOW
    if fits and 2 * sent >= sp_count * local_len:
        return gathered_layer(query_rows, key_rows, value_rows, sink_logit, operands)
    attended = window_attention(query_rows, key_rows, value_rows, sink_logit)
    return dispatched_layer(attended, operands)


def solution(mesh):
    placed = (
        P(("grp", "sp"), "tp"),
        P(("grp", "sp"), "tp"),
        P(("grp", "sp"), "tp"),
        P("tp"),
        P("tp", None),
        P(("grp", "sp", "tp"), None),
        P(),
        P(("grp", "sp", "tp"), None),
        P(("grp", "sp", "tp"), None),
        P(("sp", "tp"), None, None),
        P(("sp", "tp"), None, None),
        P(("sp", "tp"), None, None),
        P(None, "tp"),
        P(None, "tp"),
        P("tp", None),
    )
    return jax.shard_map(
        body, mesh=mesh, in_specs=placed, out_specs=P(("grp", "sp", "tp"), None), check_vma=False
    )
```

profile of v0, /device:TPU:0, one launch (start us, length us, event | category | flops | bytes accessed | tf_op | source)
XLA Modules:
  0.0 81.6 jit_solution(15547177754336729564)
XLA Ops:
  0.8 3.1 %collective-permute-start = (bf16[256,128]{1,0:T(8,128)(2,1)S(1)}, bf16[256,128]{1,0:T(8,128)(2,1)S(1)}, u32[]{:S(2)}, u32[]{:S(2)}) collective-permute-start(bf16[256,128]{1,0:T(8,128)(2,1)S(1)} %shard_map.146.refs_3_), channel_id=1, source_target_pairs={{0,4},{4,0},{8,12},{12,8},{1,5},{5,1},{9,13},{13,9},{2,6},{6,2},{1... | collective-permute-start | bytes 196616 | tf_op jit(solution)/shard_map/ppermute | solution.py:329
  4.7 1.3 %shard_map.145 = (bf16[128,256]{1,0:T(8,128)(2,1)S(1)}, bf16[256,2048]{1,0:T(8,128)(2,1)S(1)}, bf16[32,2048]{1,0:T(8,128)(2,1)S(1)}) custom-call(bf16[128,256]{1,0:T(8,128)(2,1)} %refs_0_.2, bf16[256,2048]{1,0:T(8,128)(2,1)} %refs_1_.3, bf16[32,2048]{1,0:T(8,128)(2,1)} %refs_2_.1), custom_call_target="tpu_custom_call" | custom-call | flops 1073741824 | tf_op jit(solution)/shard_map/pallas_call | solution.py:288
  6.2 2.5 %shard_map.147 = (f32[64,2048]{1,0:T(8,128)S(1)}, bf16[64,2048]{1,0:T(8,128)(2,1)S(1)}) custom-call(s32[2]{0:T(128)S(1)} %pad_add_fusion.refs_0_, f32[4]{0:T(128)} %refs_1_.5, bf16[128,256]{1,0:T(8,128)(2,1)S(1)} %get-tuple-element.32.refs_2_, bf16[256,128]{1,0:T(8,128)(2,1)S(1)} %shard_map.146.refs_3_, bf16[256,2048]{1,0:T(8,128)(2,1)S(1)} %get-tuple-element.33.refs_4_, ...), custom_call_target="tpu_custom_call" | custom-call | flops 1073741824 | tf_op jit(solution)/shard_map/pallas_call | solution.py:288
  8.7 1.5 %collective-permute-done.2.refs_2_ = bf16[64,2048]{1,0:T(8,128)(2,1)S(1)} collective-permute-done((bf16[64,2048]{1,0:T(8,128)(2,1)S(1)}, bf16[64,2048]{1,0:T(8,128)(2,1)S(1)}, u32[]{:S(2)}, u32[]{:S(2)}) %collective-permute-start.2) | collective-permute-done | bytes 262176 | tf_op jit(solution)/shard_map/ppermute | solution.py:317
  10.3 2.0 %collective-permute-start.3 = (bf16[32,2048]{1,0:T(8,128)(2,1)S(1)}, bf16[32,2048]{1,0:T(8,128)(2,1)S(1)}, u32[]{:S(2)}, u32[]{:S(2)}) collective-permute-start(bf16[32,2048]{1,0:T(8,128)(2,1)S(1)} %add_convert_fusion.8), channel_id=1, source_target_pairs={{0,2},{1,3},{2,0},{3,1},{4,6},{5,7},{6,4},{7,5},{8,10},{9,11},{10,... | collective-permute-start | bytes 393224 | tf_op jit(solution)/shard_map/ppermute | solution.py:317
  12.3 3.8 %collective-permute-done.3.refs_3_ = bf16[32,2048]{1,0:T(8,128)(2,1)S(1)} collective-permute-done((bf16[32,2048]{1,0:T(8,128)(2,1)S(1)}, bf16[32,2048]{1,0:T(8,128)(2,1)S(1)}, u32[]{:S(2)}, u32[]{:S(2)}) %collective-permute-start.3) | collective-permute-done | bytes 131104 | tf_op jit(solution)/shard_map/ppermute | solution.py:317
  17.3 1.8 %collective-permute-start.4 = (bf16[32,2176]{1,0:T(8,128)(2,1)S(1)}, bf16[32,2176]{1,0:T(8,128)(2,1)S(1)}, u32[]{:S(2)}, u32[]{:S(2)}) collective-permute-start(bf16[32,2176]{1,0:T(8,128)(2,1)S(1)} %get-tuple-element.37.refs_1_), channel_id=1, source_target_pairs={{0,2},{1,3},{2,0},{3,1},{4,6},{5,7},{6,4},{7,5},{8,10},{9,11},{10,... | collective-permute-start | bytes 417800 | tf_op jit(solution)/shard_map/ppermute | solution.py:317
  19.1 4.6 %collective-permute-start.10 = (bf16[32,2176]{1,0:T(8,128)(2,1)S(1)}, bf16[32,2176]{1,0:T(8,128)(2,1)S(1)}, u32[]{:S(2)}, u32[]{:S(2)}) collective-permute-start(bf16[32,2176]{1,0:T(8,128)(2,1)S(1)} %get-tuple-element.37.refs_1_), channel_id=1, source_target_pairs={{0,4},{4,0},{8,12},{12,8},{1,5},{5,1},{9,13},{13,9},{2,6},{6,2},{1... | collective-permute-start | bytes 417800 | tf_op jit(solution)/shard_map/ppermute | solution.py:322
  23.7 1.5 %collective-permute-start.18 = (bf16[32,2176]{1,0:T(8,128)(2,1)S(1)}, bf16[32,2176]{1,0:T(8,128)(2,1)S(1)}, u32[]{:S(2)}, u32[]{:S(2)}) collective-permute-start(bf16[32,2176]{1,0:T(8,128)(2,1)S(1)} %get-tuple-element.37.refs_1_), channel_id=1, source_target_pairs={{0,8},{4,12},{8,0},{12,4},{1,9},{5,13},{9,1},{13,5},{2,10},{6,14},... | collective-permute-start | bytes 417800 | tf_op jit(solution)/shard_map/ppermute | solution.py:322
  25.6 1.5 %collective-permute-start.26 = (bf16[32,2176]{1,0:T(8,128)(2,1)S(1)}, bf16[32,2176]{1,0:T(8,128)(2,1)S(1)}, u32[]{:S(2)}, u32[]{:S(2)}) collective-permute-start(bf16[32,2176]{1,0:T(8,128)(2,1)S(1)} %get-tuple-element.37.refs_1_), channel_id=1, source_target_pairs={{0,12},{4,8},{8,4},{12,0},{1,13},{5,9},{9,5},{13,1},{2,14},{6,10},... | collective-permute-start | bytes 417800 | tf_op jit(solution)/shard_map/ppermute | solution.py:322
  28.8 6.9 %collective-permute-done.18.refs_4_ = bf16[32,2176]{1,0:T(8,128)(2,1)S(1)} collective-permute-done((bf16[32,2176]{1,0:T(8,128)(2,1)S(1)}, bf16[32,2176]{1,0:T(8,128)(2,1)S(1)}, u32[]{:S(2)}, u32[]{:S(2)}) %collective-permute-start.18) | collective-permute-done | bytes 139296 | tf_op jit(solution)/shard_map/ppermute | solution.py:322
  35.7 5.0 %shard_map.149 = (f32[32,2048]{1,0:T(8,128)S(1)}, f32[32,2048]{1,0:T(8,128)S(1)}, bf16[32,2048]{1,0:T(8,128)(2,1)S(1)}, bf16[32,2048]{1,0:T(8,128)(2,1)S(1)}, bf...) custom-call(s32[1]{0:T(128)} %bitcast.5.refs_0_, ...), custom_call_target="tpu_custom_call" | custom-call | flops 2147483648 | tf_op jit(solution)/shard_map/pallas_call | solution.py:288
  41.4 2.0 %collective-permute-start.27 = (bf16[32,2176]{1,0:T(8,128)(2,1)S(1)}, bf16[32,2176]{1,0:T(8,128)(2,1)S(1)}, u32[]{:S(2)}, u32[]{:S(2)}) collective-permute-start(bf16[32,2176]{1,0:T(8,128)(2,1)S(1)} %collective-permute-done.26.refs_4_), channel_id=1, source_target_pairs={{0,2},{1,3},{2,0},{3,1},{4,6},{5,7},{6,4},{7,5},{8,10},{9,11},{10,... | collective-permute-start | bytes 417800 | tf_op jit(solution)/shard_map/ppermute | solution.py:317
  44.1 3.5 %collective-permute-done.27.refs_5_ = bf16[32,2176]{1,0:T(8,128)(2,1)S(1)} collective-permute-done((bf16[32,2176]{1,0:T(8,128)(2,1)S(1)}, bf16[32,2176]{1,0:T(8,128)(2,1)S(1)}, u32[]{:S(2)}, u32[]{:S(2)}) %collective-permute-start.27) | collective-permute-done | bytes 139296 | tf_op jit(solution)/shard_map/ppermute | solution.py:317
  48.1 1.8 %shard_map.150 = (f32[32,2048]{1,0:T(8,128)S(1)}, f32[32,2048]{1,0:T(8,128)S(1)}, bf16[32,2048]{1,0:T(8,128)(2,1)S(1)}, bf16[32,2048]{1,0:T(8,128)(2,1)S(1)}) custom-call(s32[1]{0:T(128)} %bitcast.5.refs_0_, bf16[2048,512]{1,0:T(8,128)(2,1)S(1)} %get-tuple-element.42.refs_1_, bf16[2048,512]{1,0:T(8,128)(2,1)S(1)} %get-tuple-element.43.refs_2_, ...), custom_call_target="tpu_custom_call" | custom-call | flops 1073741824 | tf_op jit(solution)/shard_map/pallas_call | solution.py:288
  50.0 1.8 %collective-permute-start.9 = (bf16[32,2048]{1,0:T(8,128)(2,1)S(1)}, bf16[32,2048]{1,0:T(8,128)(2,1)S(1)}, u32[]{:S(2)}, u32[]{:S(2)}) collective-permute-start(bf16[32,2048]{1,0:T(8,128)(2,1)S(1)} %add_convert_fusion.7), channel_id=1, source_target_pairs={{0,2},{1,3},{2,0},{3,1},{4,6},{5,7},{6,4},{7,5},{8,10},{9,11},{10,... | collective-permute-start | bytes 393224 | tf_op jit(solution)/shard_map/ppermute | solution.py:317
  51.8 1.9 %shard_map.151 = (f32[32,2048]{1,0:T(8,128)S(1)}, f32[32,2048]{1,0:T(8,128)S(1)}, bf16[32,2048]{1,0:T(8,128)(2,1)S(1)}, bf16[32,2048]{1,0:T(8,128)(2,1)S(1)}) custom-call(s32[1]{0:T(128)} %bitcast.5.refs_0_, bf16[2048,512]{1,0:T(8,128)(2,1)S(1)} %get-tuple-element.42.refs_1_, bf16[2048,512]{1,0:T(8,128)(2,1)S(1)} %get-tuple-element.43.refs_2_, ...), custom_call_target="tpu_custom_call" | custom-call | flops 1073741824 | tf_op jit(solution)/shard_map/pallas_call | solution.py:288
  54.3 1.8 %shard_map.152 = (f32[32,2048]{1,0:T(8,128)S(1)}, f32[32,2048]{1,0:T(8,128)S(1)}, bf16[32,2048]{1,0:T(8,128)(2,1)S(1)}, bf16[32,2048]{1,0:T(8,128)(2,1)S(1)}) custom-call(s32[1]{0:T(128)} %bitcast.5.refs_0_, bf16[2048,512]{1,0:T(8,128)(2,1)S(1)} %get-tuple-element.42.refs_1_, bf16[2048,512]{1,0:T(8,128)(2,1)S(1)} %get-tuple-element.43.refs_2_, ...), custom_call_target="tpu_custom_call" | custom-call | flops 1073741824 | tf_op jit(solution)/shard_map/pallas_call | solution.py:288
  58.6 5.1 %collective-permute-done.16 = bf16[32,2048]{1,0:T(8,128)(2,1)S(1)} collective-permute-done((bf16[32,2048]{1,0:T(8,128)(2,1)S(1)}, bf16[32,2048]{1,0:T(8,128)(2,1)S(1)}, u32[]{:S(2)}, u32[]{:S(2)}) %collective-permute-start.16) | collective-permute-done | bytes 131104 | tf_op jit(solution)/shard_map/ppermute | solution.py:317
  64.0 1.8 %collective-permute-start.32 = (bf16[32,2048]{1,0:T(8,128)(2,1)S(1)}, bf16[32,2048]{1,0:T(8,128)(2,1)S(1)}, u32[]{:S(2)}, u32[]{:S(2)}) collective-permute-start(bf16[32,2048]{1,0:T(8,128)(2,1)S(1)} %add_convert_fusion.2), channel_id=1, source_target_pairs={{0,2},{1,3},{2,0},{3,1},{4,6},{5,7},{6,4},{7,5},{8,10},{9,11},{10,... | collective-permute-start | bytes 393224 | tf_op jit(solution)/shard_map/ppermute | solution.py:317
  65.9 3.9 %collective-permute-done.24 = bf16[32,2048]{1,0:T(8,128)(2,1)S(1)} collective-permute-done((bf16[32,2048]{1,0:T(8,128)(2,1)S(1)}, bf16[32,2048]{1,0:T(8,128)(2,1)S(1)}, u32[]{:S(2)}, u32[]{:S(2)}) %collective-permute-start.24) | collective-permute-done | bytes 131104 | tf_op jit(solution)/shard_map/ppermute | solution.py:317
  69.9 3.4 %collective-permute-start.25 = (bf16[32,2048]{1,0:T(8,128)(2,1)S(1)}, bf16[32,2048]{1,0:T(8,128)(2,1)S(1)}, u32[]{:S(2)}, u32[]{:S(2)}) collective-permute-start(bf16[32,2048]{1,0:T(8,128)(2,1)S(1)} %add_convert_fusion.3), channel_id=1, source_target_pairs={{0,8},{4,12},{8,0},{12,4},{1,9},{5,13},{9,1},{13,5},{2,10},{6,14},... | collective-permute-start | bytes 393224 | tf_op jit(solution)/shard_map/ppermute | solution.py:322
  74.4 2.3 %collective-permute-done.17 = bf16[32,2048]{1,0:T(8,128)(2,1)S(1)} collective-permute-done((bf16[32,2048]{1,0:T(8,128)(2,1)S(1)}, bf16[32,2048]{1,0:T(8,128)(2,1)S(1)}, u32[]{:S(2)}, u32[]{:S(2)}) %collective-permute-start.17) | collective-permute-done | bytes 131104 | tf_op jit(solution)/shard_map/ppermute | solution.py:322
  76.7 4.0 %collective-permute-done.25 = bf16[32,2048]{1,0:T(8,128)(2,1)S(1)} collective-permute-done((bf16[32,2048]{1,0:T(8,128)(2,1)S(1)}, bf16[32,2048]{1,0:T(8,128)(2,1)S(1)}, u32[]{:S(2)}, u32[]{:S(2)}) %collective-permute-start.25) | collective-permute-done | bytes 131104 | tf_op jit(solution)/shard_map/ppermute | solution.py:322
  (62 shorter events, 12.4 us)
Async XLA Ops:
  10.3 5.8 %collective-permute-start.3 = (bf16[32,2048]{1,0:T(8,128)(2,1)S(1)}, bf16[32,2048]{1,0:T(8,128)(2,1)S(1)}, u32[]{:S(2)}, u32[]{:S(2)}) collective-permute-start(bf16[32,2048]{1,0:T(8,128)(2,1)S(1)} %add_convert_fusion.8), channel_id=1, source_target_pairs={{0,2},{1,3},{2,0},{3,1},{4,6},{5,7},{6,4},{7,5},{8,10},{9,11},{10,... | collective-permute-start | bytes 393224 | tf_op jit(solution)/shard_map/ppermute | solution.py:317
  17.3 7.9 %collective-permute-start.4 = (bf16[32,2176]{1,0:T(8,128)(2,1)S(1)}, bf16[32,2176]{1,0:T(8,128)(2,1)S(1)}, u32[]{:S(2)}, u32[]{:S(2)}) collective-permute-start(bf16[32,2176]{1,0:T(8,128)(2,1)S(1)} %get-tuple-element.37.refs_1_), channel_id=1, source_target_pairs={{0,2},{1,3},{2,0},{3,1},{4,6},{5,7},{6,4},{7,5},{8,10},{9,11},{10,... | collective-permute-start | bytes 417800 | tf_op jit(solution)/shard_map/ppermute | solution.py:317
  19.1 9.2 %collective-permute-start.10 = (bf16[32,2176]{1,0:T(8,128)(2,1)S(1)}, bf16[32,2176]{1,0:T(8,128)(2,1)S(1)}, u32[]{:S(2)}, u32[]{:S(2)}) collective-permute-start(bf16[32,2176]{1,0:T(8,128)(2,1)S(1)} %get-tuple-element.37.refs_1_), channel_id=1, source_target_pairs={{0,4},{4,0},{8,12},{12,8},{1,5},{5,1},{9,13},{13,9},{2,6},{6,2},{1... | collective-permute-start | bytes 417800 | tf_op jit(solution)/shard_map/ppermute | solution.py:322
  23.7 12.0 %collective-permute-start.18 = (bf16[32,2176]{1,0:T(8,128)(2,1)S(1)}, bf16[32,2176]{1,0:T(8,128)(2,1)S(1)}, u32[]{:S(2)}, u32[]{:S(2)}) collective-permute-start(bf16[32,2176]{1,0:T(8,128)(2,1)S(1)} %get-tuple-element.37.refs_1_), channel_id=1, source_target_pairs={{0,8},{4,12},{8,0},{12,4},{1,9},{5,13},{9,1},{13,5},{2,10},{6,14},... | collective-permute-start | bytes 417800 | tf_op jit(solution)/shard_map/ppermute | solution.py:322
  25.1 10.5 %collective-permute-start.5 = (bf16[32,2176]{1,0:T(8,128)(2,1)S(1)}, bf16[32,2176]{1,0:T(8,128)(2,1)S(1)}, u32[]{:S(2)}, u32[]{:S(2)}) collective-permute-start(bf16[32,2176]{1,0:T(8,128)(2,1)S(1)} %get-tuple-element.37.refs_1_), channel_id=1, source_target_pairs={{0,1},{1,0},{2,3},{3,2},{4,5},{5,4},{6,7},{7,6},{8,9},{9,8},{10,11... | collective-permute-start | bytes 417800 | tf_op jit(solution)/shard_map/ppermute | solution.py:317
  25.1 10.5 %collective-permute-start.6 = (bf16[32,2176]{1,0:T(8,128)(2,1)S(1)}, bf16[32,2176]{1,0:T(8,128)(2,1)S(1)}, u32[]{:S(2)}, u32[]{:S(2)}) collective-permute-start(bf16[32,2176]{1,0:T(8,128)(2,1)S(1)} %collective-permute-done.4.refs_2_), channel_id=1, source_target_pairs={{0,1},{1,0},{2,3},{3,2},{4,5},{5,4},{6,7},{7,6},{8,9},{9,8},{10,11... | collective-permute-start | bytes 417800 | tf_op jit(solution)/shard_map/ppermute | solution.py:317
  25.6 15.6 %collective-permute-start.26 = (bf16[32,2176]{1,0:T(8,128)(2,1)S(1)}, bf16[32,2176]{1,0:T(8,128)(2,1)S(1)}, u32[]{:S(2)}, u32[]{:S(2)}) collective-permute-start(bf16[32,2176]{1,0:T(8,128)(2,1)S(1)} %get-tuple-element.37.refs_1_), channel_id=1, source_target_pairs={{0,12},{4,8},{8,4},{12,0},{1,13},{5,9},{9,5},{13,1},{2,14},{6,10},... | collective-permute-start | bytes 417800 | tf_op jit(solution)/shard_map/ppermute | solution.py:322
  28.3 13.1 %collective-permute-start.11 = (bf16[32,2176]{1,0:T(8,128)(2,1)S(1)}, bf16[32,2176]{1,0:T(8,128)(2,1)S(1)}, u32[]{:S(2)}, u32[]{:S(2)}) collective-permute-start(bf16[32,2176]{1,0:T(8,128)(2,1)S(1)} %collective-permute-done.10.refs_4_), channel_id=1, source_target_pairs={{0,2},{1,3},{2,0},{3,1},{4,6},{5,7},{6,4},{7,5},{8,10},{9,11},{10,... | collective-permute-start | bytes 417800 | tf_op jit(solution)/shard_map/ppermute | solution.py:317
  35.6 7.7 %collective-permute-start.19 = (bf16[32,2176]{1,0:T(8,128)(2,1)S(1)}, bf16[32,2176]{1,0:T(8,128)(2,1)S(1)}, u32[]{:S(2)}, u32[]{:S(2)}) collective-permute-start(bf16[32,2176]{1,0:T(8,128)(2,1)S(1)} %collective-permute-done.18.refs_4_), channel_id=1, source_target_pairs={{0,2},{1,3},{2,0},{3,1},{4,6},{5,7},{6,4},{7,5},{8,10},{9,11},{10,... | collective-permute-start | bytes 417800 | tf_op jit(solution)/shard_map/ppermute | solution.py:317
  41.3 8.7 %collective-permute-start.20 = (bf16[32,2176]{1,0:T(8,128)(2,1)S(1)}, bf16[32,2176]{1,0:T(8,128)(2,1)S(1)}, u32[]{:S(2)}, u32[]{:S(2)}) collective-permute-start(bf16[32,2176]{1,0:T(8,128)(2,1)S(1)} %collective-permute-done.18.refs_4_), channel_id=1, source_target_pairs={{0,1},{1,0},{2,3},{3,2},{4,5},{5,4},{6,7},{7,6},{8,9},{9,8},{10,11... | collective-permute-start | bytes 417800 | tf_op jit(solution)/shard_map/ppermute | solution.py:317
  41.4 6.3 %collective-permute-start.27 = (bf16[32,2176]{1,0:T(8,128)(2,1)S(1)}, bf16[32,2176]{1,0:T(8,128)(2,1)S(1)}, u32[]{:S(2)}, u32[]{:S(2)}) collective-permute-start(bf16[32,2176]{1,0:T(8,128)(2,1)S(1)} %collective-permute-done.26.refs_4_), channel_id=1, source_target_pairs={{0,2},{1,3},{2,0},{3,1},{4,6},{5,7},{6,4},{7,5},{8,10},{9,11},{10,... | collective-permute-start | bytes 417800 | tf_op jit(solution)/shard_map/ppermute | solution.py:317
  43.5 8.3 %collective-permute-start.21 = (bf16[32,2176]{1,0:T(8,128)(2,1)S(1)}, bf16[32,2176]{1,0:T(8,128)(2,1)S(1)}, u32[]{:S(2)}, u32[]{:S(2)}) collective-permute-start(bf16[32,2176]{1,0:T(8,128)(2,1)S(1)} %collective-permute-done.19.refs_5_), channel_id=1, source_target_pairs={{0,1},{1,0},{2,3},{3,2},{4,5},{5,4},{6,7},{7,6},{8,9},{9,8},{10,11... | collective-permute-start | bytes 417800 | tf_op jit(solution)/shard_map/ppermute | solution.py:317
  43.9 9.8 %collective-permute-start.28 = (bf16[32,2176]{1,0:T(8,128)(2,1)S(1)}, bf16[32,2176]{1,0:T(8,128)(2,1)S(1)}, u32[]{:S(2)}, u32[]{:S(2)}) collective-permute-start(bf16[32,2176]{1,0:T(8,128)(2,1)S(1)} %collective-permute-done.26.refs_4_), channel_id=1, source_target_pairs={{0,1},{1,0},{2,3},{3,2},{4,5},{5,4},{6,7},{7,6},{8,9},{9,8},{10,11... | collective-permute-start | bytes 417800 | tf_op jit(solution)/shard_map/ppermute | solution.py:317
  47.6 26.8 %collective-permute-start.7 = (bf16[32,2048]{1,0:T(8,128)(2,1)S(1)}, bf16[32,2048]{1,0:T(8,128)(2,1)S(1)}, u32[]{:S(2)}, u32[]{:S(2)}) collective-permute-start(bf16[32,2048]{1,0:T(8,128)(2,1)S(1)} %get-tuple-element.39), channel_id=1, source_target_pairs={{0,1},{1,0},{2,3},{3,2},{4,5},{5,4},{6,7},{7,6},{8,9},{9,8},{10,11... | collective-permute-start | bytes 393224 | tf_op jit(solution)/shard_map/ppermute | solution.py:317
  47.6 6.6 %collective-permute-start.29 = (bf16[32,2176]{1,0:T(8,128)(2,1)S(1)}, bf16[32,2176]{1,0:T(8,128)(2,1)S(1)}, u32[]{:S(2)}, u32[]{:S(2)}) collective-permute-start(bf16[32,2176]{1,0:T(8,128)(2,1)S(1)} %collective-permute-done.27.refs_5_), channel_id=1, source_target_pairs={{0,1},{1,0},{2,3},{3,2},{4,5},{5,4},{6,7},{7,6},{8,9},{9,8},{10,11... | collective-permute-start | bytes 417800 | tf_op jit(solution)/shard_map/ppermute | solution.py:317
  50.0 24.5 %collective-permute-start.9 = (bf16[32,2048]{1,0:T(8,128)(2,1)S(1)}, bf16[32,2048]{1,0:T(8,128)(2,1)S(1)}, u32[]{:S(2)}, u32[]{:S(2)}) collective-permute-start(bf16[32,2048]{1,0:T(8,128)(2,1)S(1)} %add_convert_fusion.7), channel_id=1, source_target_pairs={{0,2},{1,3},{2,0},{3,1},{4,6},{5,7},{6,4},{7,5},{8,10},{9,11},{10,... | collective-permute-start | bytes 393224 | tf_op jit(solution)/shard_map/ppermute | solution.py:317
  56.2 7.8 %collective-permute-start.22 = (bf16[32,2048]{1,0:T(8,128)(2,1)S(1)}, bf16[32,2048]{1,0:T(8,128)(2,1)S(1)}, u32[]{:S(2)}, u32[]{:S(2)}) collective-permute-start(bf16[32,2048]{1,0:T(8,128)(2,1)S(1)} %get-tuple-element.50), channel_id=1, source_target_pairs={{0,1},{1,0},{2,3},{3,2},{4,5},{5,4},{6,7},{7,6},{8,9},{9,8},{10,11... | collective-permute-start | bytes 393224 | tf_op jit(solution)/shard_map/ppermute | solution.py:317
  58.1 5.6 %collective-permute-start.16 = (bf16[32,2048]{1,0:T(8,128)(2,1)S(1)}, bf16[32,2048]{1,0:T(8,128)(2,1)S(1)}, u32[]{:S(2)}, u32[]{:S(2)}) collective-permute-start(bf16[32,2048]{1,0:T(8,128)(2,1)S(1)} %add_convert_fusion.6), channel_id=1, source_target_pairs={{0,2},{1,3},{2,0},{3,1},{4,6},{5,7},{6,4},{7,5},{8,10},{9,11},{10,... | collective-permute-start | bytes 393224 | tf_op jit(solution)/shard_map/ppermute | solution.py:317
  58.5 11.4 %collective-permute-start.30 = (bf16[32,2048]{1,0:T(8,128)(2,1)S(1)}, bf16[32,2048]{1,0:T(8,128)(2,1)S(1)}, u32[]{:S(2)}, u32[]{:S(2)}) collective-permute-start(bf16[32,2048]{1,0:T(8,128)(2,1)S(1)} %get-tuple-element.54), channel_id=1, source_target_pairs={{0,1},{1,0},{2,3},{3,2},{4,5},{5,4},{6,7},{7,6},{8,9},{9,8},{10,11... | collective-permute-start | bytes 393224 | tf_op jit(solution)/shard_map/ppermute | solution.py:317
  63.7 6.1 %collective-permute-start.24 = (bf16[32,2048]{1,0:T(8,128)(2,1)S(1)}, bf16[32,2048]{1,0:T(8,128)(2,1)S(1)}, u32[]{:S(2)}, u32[]{:S(2)}) collective-permute-start(bf16[32,2048]{1,0:T(8,128)(2,1)S(1)} %add_convert_fusion.4), channel_id=1, source_target_pairs={{0,2},{1,3},{2,0},{3,1},{4,6},{5,7},{6,4},{7,5},{8,10},{9,11},{10,... | collective-permute-start | bytes 393224 | tf_op jit(solution)/shard_map/ppermute | solution.py:317
  64.0 9.3 %collective-permute-start.32 = (bf16[32,2048]{1,0:T(8,128)(2,1)S(1)}, bf16[32,2048]{1,0:T(8,128)(2,1)S(1)}, u32[]{:S(2)}, u32[]{:S(2)}) collective-permute-start(bf16[32,2048]{1,0:T(8,128)(2,1)S(1)} %add_convert_fusion.2), channel_id=1, source_target_pairs={{0,2},{1,3},{2,0},{3,1},{4,6},{5,7},{6,4},{7,5},{8,10},{9,11},{10,... | collective-permute-start | bytes 393224 | tf_op jit(solution)/shard_map/ppermute | solution.py:317
  69.8 6.9 %collective-permute-start.17 = (bf16[32,2048]{1,0:T(8,128)(2,1)S(1)}, bf16[32,2048]{1,0:T(8,128)(2,1)S(1)}, u32[]{:S(2)}, u32[]{:S(2)}) collective-permute-start(bf16[32,2048]{1,0:T(8,128)(2,1)S(1)} %add_convert_fusion.5), channel_id=1, source_target_pairs={{0,4},{4,0},{8,12},{12,8},{1,5},{5,1},{9,13},{13,9},{2,6},{6,2},{1... | collective-permute-start | bytes 393224 | tf_op jit(solution)/shard_map/ppermute | solution.py:322
  69.9 10.9 %collective-permute-start.25 = (bf16[32,2048]{1,0:T(8,128)(2,1)S(1)}, bf16[32,2048]{1,0:T(8,128)(2,1)S(1)}, u32[]{:S(2)}, u32[]{:S(2)}) collective-permute-start(bf16[32,2048]{1,0:T(8,128)(2,1)S(1)} %add_convert_fusion.3), channel_id=1, source_target_pairs={{0,8},{4,12},{8,0},{12,4},{1,9},{5,13},{9,1},{13,5},{2,10},{6,14},... | collective-permute-start | bytes 393224 | tf_op jit(solution)/shard_map/ppermute | solution.py:322
  73.4 7.4 %collective-permute-start.33 = (bf16[32,2048]{1,0:T(8,128)(2,1)S(1)}, bf16[32,2048]{1,0:T(8,128)(2,1)S(1)}, u32[]{:S(2)}, u32[]{:S(2)}) collective-permute-start(bf16[32,2048]{1,0:T(8,128)(2,1)S(1)} %add_convert_fusion.1), channel_id=1, source_target_pairs={{0,12},{4,8},{8,4},{12,0},{1,13},{5,9},{9,5},{13,1},{2,14},{6,10},... | collective-permute-start | bytes 393224 | tf_op jit(solution)/shard_map/ppermute | solution.py:322
  (10 other events, 32.5 us)
where the time goes:
time: 81.8 us; the launch traced here: 81.6 us
  waiting for transfers between devices  33.7 us (41%)
  starting transfers between devices  30.1 us (37%)
  Pallas kernels  16.3 us (20%)
  other arithmetic  1.17 us (1%)
    ppermute x26, waiting for transfers between devices, flip(): return lax.ppermute(value, 'tp', [(i, i ^ bit) for i in range(count)])  19.2 us
    pallas_call x8, Pallas kernels, on_core(): pl.pallas_call(run, out_shape=tuple(outs), in_specs=[pl.BlockSpec(memory_...  16.3 us
    ppermute x6, waiting for transfers between devices, swap(): return lax.ppermute(value, 'sp', [(i, i ^ bits) for i in range(count)])  14.3 us
    ppermute x26, starting transfers between devices, flip(): return lax.ppermute(value, 'tp', [(i, i ^ bit) for i in range(count)])  14.3 us
    ppermute x6, starting transfers between devices, swap(): return lax.ppermute(value, 'sp', [(i, i ^ bits) for i in range(count)])  12 us
    ppermute x1, starting transfers between devices, neighbours(): from_even = lax.ppermute(value, 'sp', even)  3.12 us
  transfers between devices with their start and end apart: 34, of which 11 were waited for; matrix products, arithmetic and copies ran while one was open for 0% of the time, Pallas kernels for 15%

commit v1 on v0

--- a/solution.py
+++ b/solution.py
@@ -141,7 +141,12 @@
 
 
 def fill_kernel(given, sources, results, arrival):
-    for copy in fetch(sources, results, arrival):
+    copies = fetch(sources, results, arrival)
+    if given:
+        sinks_ref = results[-1]
+        for head in range(sinks_ref.shape[0]):
+            sinks_ref[head : head + 1] = jnp.full((1, sinks_ref.shape[1]), given[0][head])
+    for copy in copies:
         copy.wait()
 
 
@@ -152,15 +157,13 @@
 
 
 def attention_kernel(total_len, given, sources, results, arrival):
-    place_ref, sink_ref, query_ref, pack_ref, weight_ref = given
-    kept_ref, sent_ref, attended_ref, *packs = results
-    packs = [pack_ref, *packs]
+    query_ref, weight_ref, sinks_ref, *packs = given
+    kept_ref, sent_ref, attended_ref = results
     rows = query_ref.shape[0]
-    copies = fetch(sources, packs[1:], arrival)
     heads = query_ref.shape[1] // HEAD
-    kv_heads = pack_ref.shape[1] // HEAD
+    kv_heads = packs[0].shape[1] // HEAD
     grouped = heads // kv_heads
-    here, me = place_ref[0], place_ref[1]
+    here, me = lax.axis_index("sp"), lax.axis_index("tp")
     span = (grouped * rows, 3 * rows)
     row = lax.broadcasted_iota(jnp.int32, span, 0)
     col = lax.broadcasted_iota(jnp.int32, span, 1)
@@ -169,8 +172,6 @@
     query_pos = here * rows + row % rows
     near = (jnp.abs(key_pos - query_pos) <= WINDOW) & (key_pos >= 0) & (key_pos < total_len)
     head_of = row[:, :1] // rows
-    for copy in copies:
-        copy.wait()
     keys = jnp.concatenate([pack[:rows] for pack in packs], axis=0)
     values = jnp.concatenate([pack[rows:] for pack in packs], axis=0)
     for group in range(kv_heads):
@@ -187,9 +188,10 @@
             queries, keys[:, lanes], (((1,), (1,)), ((), ())), preferred_element_type=jnp.float32
         )
         scores = jnp.where(near, scores * HEAD ** (-0.5), -jnp.inf)
-        sink = jnp.full(head_of.shape, sink_ref[first_head], jnp.float32)
+        sink = jnp.broadcast_to(sinks_ref[first_head : first_head + 1, :1], head_of.shape)
         for offset in range(1, grouped):
-            sink = jnp.where(head_of == offset, sink_ref[first_head + offset], sink)
+            head = first_head + offset
+            sink = jnp.where(head_of == offset, sinks_ref[head : head + 1, :1], sink)
         row_max = jnp.maximum(sink, jnp.max(scores, axis=1, keepdims=True))
         shifted = jnp.exp(scores - row_max)
         denominator = jnp.exp(sink - row_max) + jnp.sum(shifted, axis=1, keepdims=True)
@@ -212,11 +214,8 @@
 
 
 def norm_kernel(experts_all, given, sources, results, arrival):
-    stream_ref, payload_ref = results[:2]
-    for copy in fetch(sources, results[2:], arrival):
-        copy.wait()
-    residual = given[0]
-    kept, sibling, peer, gain, routes, gates = results[2:]
+    stream_ref, payload_ref = results
+    residual, gain, routes, gates, kept, sibling, peer = given
     rows, width = residual.shape
     stream = residual[...].astype(jnp.float32) + kept[:rows]
     stream = stream + sibling[:rows].astype(jnp.float32) + peer[...].astype(jnp.float32)
@@ -235,40 +234,31 @@
     payload_ref[:, width:] = spread.T.astype(jnp.bfloat16)
 
 
-def slab_kernel(experts_all, given, sources, results, arrival):
-    outs, refs = results[:4], results[4:]
-    count = sources[0].shape[0]
-    expert_ref, slab_ref = given[0], refs[-1]
-    weights = given[1:] if len(given) > 1 else refs[:3]
-    shared = refs[3:-1]
-    pieces = [slab_ref.at[pl.ds(index * count, count)] for index in range(4)]
-    copies = fetch(sources, [*pieces, *refs[:-1]], arrival)
-    for copy in copies[:4]:
-        copy.wait()
-    coming = copies[4:]
-    width = outs[0].shape[1]
+def slab_kernel(tp_count, experts_all, given, sources, results, arrival):
+    kept_ref, kept_cross_ref, sent_ref, slab_ref = results
+    pieces, weights, shared = given[:4], given[4:7], given[7:]
+    count, width = kept_ref.shape
+    for index, piece in enumerate(pieces):
+        slab_ref[index * count : (index + 1) * count] = piece[...]
+    expert = lax.axis_index("sp") * tp_count + lax.axis_index("tp")
     rows = slab_ref[:, :width]
     tail = slab_ref[:, width:].astype(jnp.float32)
     lane = lax.broadcasted_iota(jnp.int32, tail.shape, 1)
-    mine = (lane == expert_ref[0]) | (lane == expert_ref[0] + experts_all)
+    mine = (lane == expert) | (lane == expert + experts_all)
     weight = jnp.sum(jnp.where(mine, tail, 0.0), axis=1, keepdims=True)
 
-    def arrived(ref):
-        if coming:
-            coming.pop(0).wait()
-        return ref[...]
-
     def ffn(gate, up, down):
-        gate_part = dot32(rows, arrived(gate))
-        up_part = dot32(rows, arrived(up))
+        gate_part = dot32(rows, gate[...])
+        up_part = dot32(rows, up[...])
         hidden = (gate_part / (1.0 + jnp.exp(-gate_part)) * up_part).astype(jnp.bfloat16)
-        return dot32(hidden, arrived(down)).astype(jnp.bfloat16).astype(jnp.float32)
+        return dot32(hidden, down[...]).astype(jnp.bfloat16).astype(jnp.float32)
 
     part = weight * ffn(*weights)
     if shared:
         part = part + ffn(*shared)
-    for index, out in enumerate(outs):
-        out[...] = part[index * count : (index + 1) * count].astype(out.dtype)
+    kept_ref[...] = part[:count]
+    kept_cross_ref[...] = part[count : 2 * count]
+    sent_ref[...] = part[2 * count :].astype(jnp.bfloat16)
 
 
 def on_core(kernel, work, outs, smem, placed, fetched, scratch=(), arguments=()):
@@ -292,7 +282,7 @@
         + [in_vmem] * len(placed)
         + [pl.BlockSpec(memory_space=pl.ANY)] * len(fetched),
         out_specs=tuple(in_vmem for _ in outs),
-        scratch_shapes=[*scratch, pltpu.SemaphoreType.DMA((len(fetched),))],
+        scratch_shapes=[*scratch, pltpu.SemaphoreType.DMA((max(len(fetched), 1),))],
         compiler_params=pltpu.CompilerParams(vmem_limit_bytes=VMEM_BYTES),
         cost_estimate=pl.CostEstimate(flops=work, transcendentals=0, bytes_accessed=0),
     )(*smem, *placed, *fetched)
@@ -336,7 +326,6 @@
     count, width = residual.shape
     sp_count = lax.axis_size("sp")
     experts_all = sp_count * lax.axis_size("tp")
-    here, me = lax.axis_index("sp"), lax.axis_index("tp")
     f32, bf16 = jnp.float32, jnp.bfloat16
 
     def held(rows, columns, dtype):
@@ -352,79 +341,69 @@
         [key_rows, value_rows],
         arguments=(0, 1),
     )
-    wanted = [query_rows, out_weight, residual]
-    query_here, out_here, residual_here = on_core(
-        fill_kernel, SLAB_WORK, [room(array) for array in wanted], [], [], wanted,
-        arguments=(0, 1, 2),
-    )
+    wanted = [query_rows, out_weight, residual, norm_gain.reshape(1, width)]
+    wanted += [routes.T, gate_weights.T, expert_gate[0], expert_up[0], expert_down[0]]
+    wanted += [shared_gate, shared_up, shared_down]
+    query_here, out_here, *filled = on_core(
+        fill_kernel,
+        FILL_WORK,
+        [*[room(array) for array in wanted], pltpu.VMEM((sink_logit.shape[0], LANES), f32)],
+        [pltpu.with_memory_space_constraint(sink_logit, pltpu.HBM)],
+        [],
+        wanted,
+        arguments=range(len(wanted)),
+    )
+    terms, weights, shared, sinks = filled[:4], filled[4:7], filled[7:10], filled[10]
 
     kept, sent = on_core(
         functools.partial(attention_kernel, sp_count * local_len),
         SLAB_WORK,
         [held(2 * count, width, f32), held(2 * count, width, bf16)],
-        [
-            jnp.stack([here, me]).astype(jnp.int32),
-            pltpu.with_memory_space_constraint(sink_logit, pltpu.HBM),
-        ],
-        [query_here, pack, out_here],
-        neighbours(pack),
-        [room(query_rows)] + [pltpu.VMEM((2 * local_len, kv_width), bf16)] * 2,
+        [],
+        [query_here, out_here, sinks, pack, *neighbours(pack)],
+        [],
+        [room(query_rows)],
     )
     sibling = flip(sent, 1)
     peer = flip((kept[count:] + sibling[count:].astype(f32)).astype(bf16), 2)
     tail = 2 * experts_all + -(2 * experts_all) % LANES
-    terms = [kept, sibling, peer, norm_gain.reshape(1, width), routes.T, gate_weights.T]
     stream, payload = on_core(
         functools.partial(norm_kernel, experts_all),
         SLAB_WORK // 2,
         [held(count, width, f32), held(count, width + tail, bf16)],
         [],
-        [residual_here],
-        terms,
-        [room(term) for term in terms],
-        (3, 4, 5),
-    )
-
-    expert = (here * lax.axis_size("tp") + me).reshape(1).astype(jnp.int32)
-    halves = [held(count, width, f32)] * 2 + [held(count, width, bf16)] * 2
-
-    experts = [expert_gate[0], expert_up[0], expert_down[0]]
-    shared = [shared_gate, shared_up, shared_down]
+        [*terms, kept, sibling, peer],
+        [],
+    )
+
+    halves = [held(count, width, f32)] * 2 + [held(2 * count, width, bf16)]
+
     slab_room = pltpu.VMEM((4 * count, width + tail), bf16)
 
     def pieces_of(rows):
         crossed = flip(rows, 2)
         return [rows, crossed, flip(rows, 1), flip(crossed, 1)]
 
-    def returned(kept, kept_cross, sent, sent_cross):
-        sent_cross = flip(sent_cross, 1)
-        kept_cross = (kept_cross + sent_cross.astype(f32)).astype(bf16)
-        sent = flip(sent, 1)
-        return kept + sent.astype(f32) + flip(kept_cross, 2).astype(f32)
-
-    kernel = functools.partial(slab_kernel, experts_all)
-    *own, gate, up, down = on_core(
-        kernel,
-        FILL_WORK,
-        halves + [room(array) for array in experts],
-        [expert],
-        [],
-        [*pieces_of(payload), *experts, *shared],
-        [*[room(array) for array in shared], slab_room],
-        range(4, 10),
-    )
-    total = stream + returned(*own)
-    for step in range(1, sp_count):
+    def returned(kept, kept_cross, sent):
+        sent = flip(sent, 1).astype(f32)
+        kept_cross = (kept_cross + sent[count:]).astype(bf16)
+        return kept + sent[:count] + flip(kept_cross, 2).astype(f32)
+
+    def through_expert(rows, *shared):
         parts = on_core(
-            kernel,
+            functools.partial(slab_kernel, lax.axis_size("tp"), experts_all),
             SLAB_WORK,
             halves,
-            [expert],
-            [gate, up, down],
-            pieces_of(swap(payload, step)),
+            [],
+            [*pieces_of(rows), *weights, *shared],
+            [],
             [slab_room],
         )
-        part = returned(*parts).astype(bf16)
+        return returned(*parts)
+
+    total = stream + through_expert(payload, *shared)
+    for step in range(1, sp_count):
+        part = through_expert(swap(payload, step)).astype(bf16)
         total = total + swap(part, step).astype(f32)
     return total.astype(bf16)
 

time: 81.8 us -> 73.4 us (0.90)
  Pallas kernels: 16.3 us -> 12.8 us
  starting transfers between devices: 30.1 us -> 26.9 us
  waiting for transfers between devices: 33.7 us -> 32.2 us
    pallas_call x8, Pallas kernels: 16.3 us -> 12.8 us  [on_core(): pl.pallas_call(run, out_shape=tuple(outs), in_specs=[pl.BlockSpec(memory_...]
    ppermute x6, starting transfers between devices: 12 us -> 9.63 us  [swap(): return lax.ppermute(value, 'sp', [(i, i ^ bits) for i in range(count)])]
    ppermute x26 -> x22, waiting for transfers between devices: 19.2 us -> 18 us  [flip(): return lax.ppermute(value, 'tp', [(i, i ^ bit) for i in range(count)])]
    ppermute x26 -> x22, starting transfers between devices: 14.3 us -> 13.5 us  [flip(): return lax.ppermute(value, 'tp', [(i, i ^ bit) for i in range(count)])]
  transfers between devices with their start and end apart: 34 -> 30, of which waited for: 11 -> 8; matrix products, arithmetic and copies ran while one was open for 0% -> 1% of each run, Pallas kernels for 15% -> 13%
where the time goes in v1:
time: 73.4 us; the launch traced here: 73.2 us
  waiting for transfers between devices  32.2 us (44%)
  starting transfers between devices  26.9 us (37%)
  Pallas kernels  12.8 us (17%)
  other arithmetic  1.23 us (2%)
    ppermute x22, waiting for transfers between devices, flip(): return lax.ppermute(value, 'tp', [(i, i ^ bit) for i in range(count)])  18 us
    ppermute x6, waiting for transfers between devices, swap(): return lax.ppermute(value, 'sp', [(i, i ^ bits) for i in range(count)])  14.2 us
    ppermute x22, starting transfers between devices, flip(): return lax.ppermute(value, 'tp', [(i, i ^ bit) for i in range(count)])  13.5 us
    pallas_call x8, Pallas kernels, on_core(): pl.pallas_call(run, out_shape=tuple(outs), in_specs=[pl.BlockSpec(memory_...  12.8 us
    ppermute x6, starting transfers between devices, swap(): return lax.ppermute(value, 'sp', [(i, i ^ bits) for i in range(count)])  9.63 us
    ppermute x1, starting transfers between devices, neighbours(): from_even = lax.ppermute(value, 'sp', even)  3.12 us
  transfers between devices with their start and end apart: 30, of which 8 were waited for; matrix products, arithmetic and copies ran while one was open for 1% of the time, Pallas kernels for 13%

profile of v1, /device:TPU:0, one launch (start us, length us, event | category | flops | bytes accessed | tf_op | source)
XLA Modules:
  0.0 73.2 jit_solution(1918508703854350444)
XLA Ops:
  0.8 3.1 %collective-permute-start = (bf16[256,128]{1,0:T(8,128)(2,1)S(1)}, bf16[256,128]{1,0:T(8,128)(2,1)S(1)}, u32[]{:S(2)}, u32[]{:S(2)}) collective-permute-start(bf16[256,128]{1,0:T(8,128)(2,1)S(1)} %shard_map.146.refs_3_), channel_id=1, source_target_pairs={{0,4},{4,0},{8,12},{12,8},{1,5},{5,1},{9,13},{13,9},{2,6},{6,2},{1... | collective-permute-start | bytes 196616 | tf_op jit(solution)/shard_map/ppermute | solution.py:319
  4.6 4.4 %shard_map.145 = (bf16[128,256]{1,0:T(8,128)(2,1)S(1)}, bf16[256,2048]{1,0:T(8,128)(2,1)S(1)}, bf16[32,2048]{1,0:T(8,128)(2,1)S(1)}, f32[1,2048]{1,0:T(1,128)S(1...) custom-call(f32[4]{0:T(128)} %refs_0_.2, ...), custom_call_target="tpu_custom_call" | custom-call | flops 2147483648 | tf_op jit(solution)/shard_map/pallas_call | solution.py:278
  9.0 2.3 %shard_map.147 = (f32[64,2048]{1,0:T(8,128)S(1)}, bf16[64,2048]{1,0:T(8,128)(2,1)S(1)}) custom-call(bf16[128,256]{1,0:T(8,128)(2,1)S(1)} %get-tuple-element.38.refs_0_, bf16[256,2048]{1,0:T(8,128)(2,1)S(1)} %get-tuple-element.39.refs_1_, f32[4,128]{1,0:T(4,128)S(1)} %get-tuple-element.40.refs_2_, bf16[256,128]{1,0:T(8,128)(2,1)S(1)} %shard_map.146.refs_3_, ...), custom_call_target="tpu_custom_call" | custom-call | flops 1073741824 | tf_op jit(solution)/shard_map/pallas_call | solution.py:278
  11.4 1.5 %collective-permute-done.2.refs_5_ = bf16[64,2048]{1,0:T(8,128)(2,1)S(1)} collective-permute-done((bf16[64,2048]{1,0:T(8,128)(2,1)S(1)}, bf16[64,2048]{1,0:T(8,128)(2,1)S(1)}, u32[]{:S(2)}, u32[]{:S(2)}) %collective-permute-start.2) | collective-permute-done | bytes 262176 | tf_op jit(solution)/shard_map/ppermute | solution.py:307
  13.0 1.6 %collective-permute-start.3 = (bf16[32,2048]{1,0:T(8,128)(2,1)S(1)}, bf16[32,2048]{1,0:T(8,128)(2,1)S(1)}, u32[]{:S(2)}, u32[]{:S(2)}) collective-permute-start(bf16[32,2048]{1,0:T(8,128)(2,1)S(1)} %add_convert_fusion), channel_id=1, source_target_pairs={{0,2},{1,3},{2,0},{3,1},{4,6},{5,7},{6,4},{7,5},{8,10},{9,11},{10,... | collective-permute-start | bytes 393224 | tf_op jit(solution)/shard_map/ppermute | solution.py:307
  14.6 4.0 %collective-permute-done.3.refs_6_ = bf16[32,2048]{1,0:T(8,128)(2,1)S(1)} collective-permute-done((bf16[32,2048]{1,0:T(8,128)(2,1)S(1)}, bf16[32,2048]{1,0:T(8,128)(2,1)S(1)}, u32[]{:S(2)}, u32[]{:S(2)}) %collective-permute-start.3) | collective-permute-done | bytes 131104 | tf_op jit(solution)/shard_map/ppermute | solution.py:307
  18.8 4.5 %collective-permute-start.9 = (bf16[32,2176]{1,0:T(8,128)(2,1)S(1)}, bf16[32,2176]{1,0:T(8,128)(2,1)S(1)}, u32[]{:S(2)}, u32[]{:S(2)}) collective-permute-start(bf16[32,2176]{1,0:T(8,128)(2,1)S(1)} %get-tuple-element.44.refs_0_), channel_id=1, source_target_pairs={{0,4},{4,0},{8,12},{12,8},{1,5},{5,1},{9,13},{13,9},{2,6},{6,2},{1... | collective-permute-start | bytes 417800 | tf_op jit(solution)/shard_map/ppermute | solution.py:312
  23.3 1.5 %collective-permute-start.4 = (bf16[32,2176]{1,0:T(8,128)(2,1)S(1)}, bf16[32,2176]{1,0:T(8,128)(2,1)S(1)}, u32[]{:S(2)}, u32[]{:S(2)}) collective-permute-start(bf16[32,2176]{1,0:T(8,128)(2,1)S(1)} %get-tuple-element.44.refs_0_), channel_id=1, source_target_pairs={{0,2},{1,3},{2,0},{3,1},{4,6},{5,7},{6,4},{7,5},{8,10},{9,11},{10,... | collective-permute-start | bytes 417800 | tf_op jit(solution)/shard_map/ppermute | solution.py:307
  24.8 2.4 %collective-permute-start.23 = (bf16[32,2176]{1,0:T(8,128)(2,1)S(1)}, bf16[32,2176]{1,0:T(8,128)(2,1)S(1)}, u32[]{:S(2)}, u32[]{:S(2)}) collective-permute-start(bf16[32,2176]{1,0:T(8,128)(2,1)S(1)} %get-tuple-element.44.refs_0_), channel_id=1, source_target_pairs={{0,12},{4,8},{8,4},{12,0},{1,13},{5,9},{9,5},{13,1},{2,14},{6,10},... | collective-permute-start | bytes 417800 | tf_op jit(solution)/shard_map/ppermute | solution.py:312
  27.2 1.6 %collective-permute-start.10 = (bf16[32,2176]{1,0:T(8,128)(2,1)S(1)}, bf16[32,2176]{1,0:T(8,128)(2,1)S(1)}, u32[]{:S(2)}, u32[]{:S(2)}) collective-permute-start(bf16[32,2176]{1,0:T(8,128)(2,1)S(1)} %collective-permute-done.9.refs_0_), channel_id=1, source_target_pairs={{0,2},{1,3},{2,0},{3,1},{4,6},{5,7},{6,4},{7,5},{8,10},{9,11},{10,... | collective-permute-start | bytes 417800 | tf_op jit(solution)/shard_map/ppermute | solution.py:307
  28.8 7.4 %collective-permute-done.16.refs_0_ = bf16[32,2176]{1,0:T(8,128)(2,1)S(1)} collective-permute-done((bf16[32,2176]{1,0:T(8,128)(2,1)S(1)}, bf16[32,2176]{1,0:T(8,128)(2,1)S(1)}, u32[]{:S(2)}, u32[]{:S(2)}) %collective-permute-start.16) | collective-permute-done | bytes 139296 | tf_op jit(solution)/shard_map/ppermute | solution.py:312
  36.2 1.2 %collective-permute-start.17 = (bf16[32,2176]{1,0:T(8,128)(2,1)S(1)}, bf16[32,2176]{1,0:T(8,128)(2,1)S(1)}, u32[]{:S(2)}, u32[]{:S(2)}) collective-permute-start(bf16[32,2176]{1,0:T(8,128)(2,1)S(1)} %collective-permute-done.16.refs_0_), channel_id=1, source_target_pairs={{0,2},{1,3},{2,0},{3,1},{4,6},{5,7},{6,4},{7,5},{8,10},{9,11},{10,... | collective-permute-start | bytes 417800 | tf_op jit(solution)/shard_map/ppermute | solution.py:307
  38.9 3.2 %collective-permute-done.17.refs_1_ = bf16[32,2176]{1,0:T(8,128)(2,1)S(1)} collective-permute-done((bf16[32,2176]{1,0:T(8,128)(2,1)S(1)}, bf16[32,2176]{1,0:T(8,128)(2,1)S(1)}, u32[]{:S(2)}, u32[]{:S(2)}) %collective-permute-start.17) | collective-permute-done | bytes 139296 | tf_op jit(solution)/shard_map/ppermute | solution.py:307
  42.0 1.7 %shard_map.149 = (f32[32,2048]{1,0:T(8,128)S(1)}, f32[32,2048]{1,0:T(8,128)S(1)}, bf16[64,2048]{1,0:T(8,128)(2,1)S(1)}) custom-call(bf16[32,2176]{1,0:T(8,128)(2,1)S(1)} %get-tuple-element.44.refs_0_, bf16[32,2176]{1,0:T(8,128)(2,1)S(1)} %collective-permute-done.4.refs_1_, bf16[32,2176]{1,0:T(8,128)(2,1)S(1)} %collective-permute-done.5.refs_2_, ...), custom_call_target="tpu_custom_call" | custom-call | flops 1073741824 | tf_op jit(solution)/shard_map/pallas_call | solution.py:278
  44.8 1.1 %shard_map.150 = (f32[32,2048]{1,0:T(8,128)S(1)}, f32[32,2048]{1,0:T(8,128)S(1)}, bf16[64,2048]{1,0:T(8,128)(2,1)S(1)}) custom-call(bf16[32,2176]{1,0:T(8,128)(2,1)S(1)} %collective-permute-done.9.refs_0_, bf16[32,2176]{1,0:T(8,128)(2,1)S(1)} %collective-permute-done.10.refs_1_, bf16[32,2176]{1,0:T(8,128)(2,1)S(1)} %collective-permute-done.11.refs_2_, ...), custom_call_target="tpu_custom_call" | custom-call | flops 1073741824 | tf_op jit(solution)/shard_map/pallas_call | solution.py:278
  46.1 1.1 %shard_map.151 = (f32[32,2048]{1,0:T(8,128)S(1)}, f32[32,2048]{1,0:T(8,128)S(1)}, bf16[64,2048]{1,0:T(8,128)(2,1)S(1)}) custom-call(bf16[32,2176]{1,0:T(8,128)(2,1)S(1)} %collective-permute-done.16.refs_0_, bf16[32,2176]{1,0:T(8,128)(2,1)S(1)} %collective-permute-done.17.refs_1_, bf16[32,2176]{1,0:T(8,128)(2,1)S(1)} %collective-permute-done.18.refs_2_, ...), custom_call_target="tpu_custom_call" | custom-call | flops 1073741824 | tf_op jit(solution)/shard_map/pallas_call | solution.py:278
  47.7 1.1 %shard_map.152 = (f32[32,2048]{1,0:T(8,128)S(1)}, f32[32,2048]{1,0:T(8,128)S(1)}, bf16[64,2048]{1,0:T(8,128)(2,1)S(1)}) custom-call(bf16[32,2176]{1,0:T(8,128)(2,1)S(1)} %collective-permute-done.23.refs_0_, bf16[32,2176]{1,0:T(8,128)(2,1)S(1)} %collective-permute-done.24.refs_1_, bf16[32,2176]{1,0:T(8,128)(2,1)S(1)} %collective-permute-done.25.refs_2_, ...), custom_call_target="tpu_custom_call" | custom-call | flops 1073741824 | tf_op jit(solution)/shard_map/pallas_call | solution.py:278
  49.1 1.7 %collective-permute-start.8 = (bf16[32,2048]{1,0:T(8,128)(2,1)S(1)}, bf16[32,2048]{1,0:T(8,128)(2,1)S(1)}, u32[]{:S(2)}, u32[]{:S(2)}) collective-permute-start(bf16[32,2048]{1,0:T(8,128)(2,1)S(1)} %fusion.9), channel_id=1, source_target_pairs={{0,2},{1,3},{2,0},{3,1},{4,6},{5,7},{6,4},{7,5},{8,10},{9,11},{10,... | collective-permute-start | bytes 393224 | tf_op jit(solution)/shard_map/ppermute | solution.py:307
  51.4 1.7 %collective-permute-start.21 = (bf16[32,2048]{1,0:T(8,128)(2,1)S(1)}, bf16[32,2048]{1,0:T(8,128)(2,1)S(1)}, u32[]{:S(2)}, u32[]{:S(2)}) collective-permute-start(bf16[32,2048]{1,0:T(8,128)(2,1)S(1)} %fusion.3), channel_id=1, source_target_pairs={{0,2},{1,3},{2,0},{3,1},{4,6},{5,7},{6,4},{7,5},{8,10},{9,11},{10,... | collective-permute-start | bytes 393224 | tf_op jit(solution)/shard_map/ppermute | solution.py:307
  53.6 4.7 %collective-permute-done.14 = bf16[32,2048]{1,0:T(8,128)(2,1)S(1)} collective-permute-done((bf16[32,2048]{1,0:T(8,128)(2,1)S(1)}, bf16[32,2048]{1,0:T(8,128)(2,1)S(1)}, u32[]{:S(2)}, u32[]{:S(2)}) %collective-permute-start.14) | collective-permute-done | bytes 131104 | tf_op jit(solution)/shard_map/ppermute | solution.py:307
  58.7 2.4 %collective-permute-done.21 = bf16[32,2048]{1,0:T(8,128)(2,1)S(1)} collective-permute-done((bf16[32,2048]{1,0:T(8,128)(2,1)S(1)}, bf16[32,2048]{1,0:T(8,128)(2,1)S(1)}, u32[]{:S(2)}, u32[]{:S(2)}) %collective-permute-start.21) | collective-permute-done | bytes 131104 | tf_op jit(solution)/shard_map/ppermute | solution.py:307
  61.3 2.1 %collective-permute-done.28 = bf16[32,2048]{1,0:T(8,128)(2,1)S(1)} collective-permute-done((bf16[32,2048]{1,0:T(8,128)(2,1)S(1)}, bf16[32,2048]{1,0:T(8,128)(2,1)S(1)}, u32[]{:S(2)}, u32[]{:S(2)}) %collective-permute-start.28) | collective-permute-done | bytes 131104 | tf_op jit(solution)/shard_map/ppermute | solution.py:307
  63.5 2.2 %collective-permute-start.29 = (bf16[32,2048]{1,0:T(8,128)(2,1)S(1)}, bf16[32,2048]{1,0:T(8,128)(2,1)S(1)}, u32[]{:S(2)}, u32[]{:S(2)}) collective-permute-start(bf16[32,2048]{1,0:T(8,128)(2,1)S(1)} %fusion.2), channel_id=1, source_target_pairs={{0,12},{4,8},{8,4},{12,0},{1,13},{5,9},{9,5},{13,1},{2,14},{6,10},... | collective-permute-start | bytes 393224 | tf_op jit(solution)/shard_map/ppermute | solution.py:312
  65.7 6.7 %collective-permute-done.22 = bf16[32,2048]{1,0:T(8,128)(2,1)S(1)} collective-permute-done((bf16[32,2048]{1,0:T(8,128)(2,1)S(1)}, bf16[32,2048]{1,0:T(8,128)(2,1)S(1)}, u32[]{:S(2)}, u32[]{:S(2)}) %collective-permute-start.22) | collective-permute-done | bytes 131104 | tf_op jit(solution)/shard_map/ppermute | solution.py:312
  (57 shorter events, 7.6 us)
Async XLA Ops:
  0.8 8.2 %collective-permute-start = (bf16[256,128]{1,0:T(8,128)(2,1)S(1)}, bf16[256,128]{1,0:T(8,128)(2,1)S(1)}, u32[]{:S(2)}, u32[]{:S(2)}) collective-permute-start(bf16[256,128]{1,0:T(8,128)(2,1)S(1)} %shard_map.146.refs_3_), channel_id=1, source_target_pairs={{0,4},{4,0},{8,12},{12,8},{1,5},{5,1},{9,13},{13,9},{2,6},{6,2},{1... | collective-permute-start | bytes 196616 | tf_op jit(solution)/shard_map/ppermute | solution.py:319
  3.9 5.1 %collective-permute-start.1 = (bf16[256,128]{1,0:T(8,128)(2,1)S(1)}, bf16[256,128]{1,0:T(8,128)(2,1)S(1)}, u32[]{:S(2)}, u32[]{:S(2)}) collective-permute-start(bf16[256,128]{1,0:T(8,128)(2,1)S(1)} %shard_map.146.refs_3_), channel_id=1, source_target_pairs={{4,8},{8,4},{5,9},{9,5},{6,10},{10,6},{7,11},{11,7},{20,24},{24,20... | collective-permute-start | bytes 196616 | tf_op jit(solution)/shard_map/ppermute | solution.py:320
  13.0 5.6 %collective-permute-start.3 = (bf16[32,2048]{1,0:T(8,128)(2,1)S(1)}, bf16[32,2048]{1,0:T(8,128)(2,1)S(1)}, u32[]{:S(2)}, u32[]{:S(2)}) collective-permute-start(bf16[32,2048]{1,0:T(8,128)(2,1)S(1)} %add_convert_fusion), channel_id=1, source_target_pairs={{0,2},{1,3},{2,0},{3,1},{4,6},{5,7},{6,4},{7,5},{8,10},{9,11},{10,... | collective-permute-start | bytes 393224 | tf_op jit(solution)/shard_map/ppermute | solution.py:307
  18.8 8.4 %collective-permute-start.9 = (bf16[32,2176]{1,0:T(8,128)(2,1)S(1)}, bf16[32,2176]{1,0:T(8,128)(2,1)S(1)}, u32[]{:S(2)}, u32[]{:S(2)}) collective-permute-start(bf16[32,2176]{1,0:T(8,128)(2,1)S(1)} %get-tuple-element.44.refs_0_), channel_id=1, source_target_pairs={{0,4},{4,0},{8,12},{12,8},{1,5},{5,1},{9,13},{13,9},{2,6},{6,2},{1... | collective-permute-start | bytes 417800 | tf_op jit(solution)/shard_map/ppermute | solution.py:312
  23.3 5.6 %collective-permute-start.4 = (bf16[32,2176]{1,0:T(8,128)(2,1)S(1)}, bf16[32,2176]{1,0:T(8,128)(2,1)S(1)}, u32[]{:S(2)}, u32[]{:S(2)}) collective-permute-start(bf16[32,2176]{1,0:T(8,128)(2,1)S(1)} %get-tuple-element.44.refs_0_), channel_id=1, source_target_pairs={{0,2},{1,3},{2,0},{3,1},{4,6},{5,7},{6,4},{7,5},{8,10},{9,11},{10,... | collective-permute-start | bytes 417800 | tf_op jit(solution)/shard_map/ppermute | solution.py:307
  24.8 11.5 %collective-permute-start.16 = (bf16[32,2176]{1,0:T(8,128)(2,1)S(1)}, bf16[32,2176]{1,0:T(8,128)(2,1)S(1)}, u32[]{:S(2)}, u32[]{:S(2)}) collective-permute-start(bf16[32,2176]{1,0:T(8,128)(2,1)S(1)} %get-tuple-element.44.refs_0_), channel_id=1, source_target_pairs={{0,8},{4,12},{8,0},{12,4},{1,9},{5,13},{9,1},{13,5},{2,10},{6,14},... | collective-permute-start | bytes 417800 | tf_op jit(solution)/shard_map/ppermute | solution.py:312
  24.8 12.7 %collective-permute-start.5 = (bf16[32,2176]{1,0:T(8,128)(2,1)S(1)}, bf16[32,2176]{1,0:T(8,128)(2,1)S(1)}, u32[]{:S(2)}, u32[]{:S(2)}) collective-permute-start(bf16[32,2176]{1,0:T(8,128)(2,1)S(1)} %get-tuple-element.44.refs_0_), channel_id=1, source_target_pairs={{0,1},{1,0},{2,3},{3,2},{4,5},{5,4},{6,7},{7,6},{8,9},{9,8},{10,11... | collective-permute-start | bytes 417800 | tf_op jit(solution)/shard_map/ppermute | solution.py:307
  24.8 12.7 %collective-permute-start.23 = (bf16[32,2176]{1,0:T(8,128)(2,1)S(1)}, bf16[32,2176]{1,0:T(8,128)(2,1)S(1)}, u32[]{:S(2)}, u32[]{:S(2)}) collective-permute-start(bf16[32,2176]{1,0:T(8,128)(2,1)S(1)} %get-tuple-element.44.refs_0_), channel_id=1, source_target_pairs={{0,12},{4,8},{8,4},{12,0},{1,13},{5,9},{9,5},{13,1},{2,14},{6,10},... | collective-permute-start | bytes 417800 | tf_op jit(solution)/shard_map/ppermute | solution.py:312
  27.2 11.2 %collective-permute-start.10 = (bf16[32,2176]{1,0:T(8,128)(2,1)S(1)}, bf16[32,2176]{1,0:T(8,128)(2,1)S(1)}, u32[]{:S(2)}, u32[]{:S(2)}) collective-permute-start(bf16[32,2176]{1,0:T(8,128)(2,1)S(1)} %collective-permute-done.9.refs_0_), channel_id=1, source_target_pairs={{0,2},{1,3},{2,0},{3,1},{4,6},{5,7},{6,4},{7,5},{8,10},{9,11},{10,... | collective-permute-start | bytes 417800 | tf_op jit(solution)/shard_map/ppermute | solution.py:307
  28.8 9.7 %collective-permute-start.6 = (bf16[32,2176]{1,0:T(8,128)(2,1)S(1)}, bf16[32,2176]{1,0:T(8,128)(2,1)S(1)}, u32[]{:S(2)}, u32[]{:S(2)}) collective-permute-start(bf16[32,2176]{1,0:T(8,128)(2,1)S(1)} %collective-permute-done.4.refs_1_), channel_id=1, source_target_pairs={{0,1},{1,0},{2,3},{3,2},{4,5},{5,4},{6,7},{7,6},{8,9},{9,8},{10,11... | collective-permute-start | bytes 417800 | tf_op jit(solution)/shard_map/ppermute | solution.py:307
  36.2 5.8 %collective-permute-start.17 = (bf16[32,2176]{1,0:T(8,128)(2,1)S(1)}, bf16[32,2176]{1,0:T(8,128)(2,1)S(1)}, u32[]{:S(2)}, u32[]{:S(2)}) collective-permute-start(bf16[32,2176]{1,0:T(8,128)(2,1)S(1)} %collective-permute-done.16.refs_0_), channel_id=1, source_target_pairs={{0,2},{1,3},{2,0},{3,1},{4,6},{5,7},{6,4},{7,5},{8,10},{9,11},{10,... | collective-permute-start | bytes 417800 | tf_op jit(solution)/shard_map/ppermute | solution.py:307
  37.5 6.2 %collective-permute-start.11 = (bf16[32,2176]{1,0:T(8,128)(2,1)S(1)}, bf16[32,2176]{1,0:T(8,128)(2,1)S(1)}, u32[]{:S(2)}, u32[]{:S(2)}) collective-permute-start(bf16[32,2176]{1,0:T(8,128)(2,1)S(1)} %collective-permute-done.9.refs_0_), channel_id=1, source_target_pairs={{0,1},{1,0},{2,3},{3,2},{4,5},{5,4},{6,7},{7,6},{8,9},{9,8},{10,11... | collective-permute-start | bytes 417800 | tf_op jit(solution)/shard_map/ppermute | solution.py:307
  37.5 6.8 %collective-permute-start.24 = (bf16[32,2176]{1,0:T(8,128)(2,1)S(1)}, bf16[32,2176]{1,0:T(8,128)(2,1)S(1)}, u32[]{:S(2)}, u32[]{:S(2)}) collective-permute-start(bf16[32,2176]{1,0:T(8,128)(2,1)S(1)} %collective-permute-done.23.refs_0_), channel_id=1, source_target_pairs={{0,2},{1,3},{2,0},{3,1},{4,6},{5,7},{6,4},{7,5},{8,10},{9,11},{10,... | collective-permute-start | bytes 417800 | tf_op jit(solution)/shard_map/ppermute | solution.py:307
  38.4 6.0 %collective-permute-start.12 = (bf16[32,2176]{1,0:T(8,128)(2,1)S(1)}, bf16[32,2176]{1,0:T(8,128)(2,1)S(1)}, u32[]{:S(2)}, u32[]{:S(2)}) collective-permute-start(bf16[32,2176]{1,0:T(8,128)(2,1)S(1)} %collective-permute-done.10.refs_1_), channel_id=1, source_target_pairs={{0,1},{1,0},{2,3},{3,2},{4,5},{5,4},{6,7},{7,6},{8,9},{9,8},{10,11... | collective-permute-start | bytes 417800 | tf_op jit(solution)/shard_map/ppermute | solution.py:307
  38.5 7.4 %collective-permute-start.18 = (bf16[32,2176]{1,0:T(8,128)(2,1)S(1)}, bf16[32,2176]{1,0:T(8,128)(2,1)S(1)}, u32[]{:S(2)}, u32[]{:S(2)}) collective-permute-start(bf16[32,2176]{1,0:T(8,128)(2,1)S(1)} %collective-permute-done.16.refs_0_), channel_id=1, source_target_pairs={{0,1},{1,0},{2,3},{3,2},{4,5},{5,4},{6,7},{7,6},{8,9},{9,8},{10,11... | collective-permute-start | bytes 417800 | tf_op jit(solution)/shard_map/ppermute | solution.py:307
  44.3 4.7 %collective-permute-start.7 = (bf16[64,2048]{1,0:T(8,128)(2,1)S(1)}, bf16[64,2048]{1,0:T(8,128)(2,1)S(1)}, u32[]{:S(2)}, u32[]{:S(2)}) collective-permute-start(bf16[64,2048]{1,0:T(8,128)(2,1)S(1)} %get-tuple-element.52), channel_id=1, source_target_pairs={{0,1},{1,0},{2,3},{3,2},{4,5},{5,4},{6,7},{7,6},{8,9},{9,8},{10,11... | collective-permute-start | bytes 786440 | tf_op jit(solution)/shard_map/ppermute | solution.py:307
  46.0 4.8 %collective-permute-start.13 = (bf16[64,2048]{1,0:T(8,128)(2,1)S(1)}, bf16[64,2048]{1,0:T(8,128)(2,1)S(1)}, u32[]{:S(2)}, u32[]{:S(2)}) collective-permute-start(bf16[64,2048]{1,0:T(8,128)(2,1)S(1)} %get-tuple-element.55), channel_id=1, source_target_pairs={{0,1},{1,0},{2,3},{3,2},{4,5},{5,4},{6,7},{7,6},{8,9},{9,8},{10,11... | collective-permute-start | bytes 786440 | tf_op jit(solution)/shard_map/ppermute | solution.py:307
  49.1 16.6 %collective-permute-start.8 = (bf16[32,2048]{1,0:T(8,128)(2,1)S(1)}, bf16[32,2048]{1,0:T(8,128)(2,1)S(1)}, u32[]{:S(2)}, u32[]{:S(2)}) collective-permute-start(bf16[32,2048]{1,0:T(8,128)(2,1)S(1)} %fusion.9), channel_id=1, source_target_pairs={{0,2},{1,3},{2,0},{3,1},{4,6},{5,7},{6,4},{7,5},{8,10},{9,11},{10,... | collective-permute-start | bytes 393224 | tf_op jit(solution)/shard_map/ppermute | solution.py:307
  50.9 7.5 %collective-permute-start.14 = (bf16[32,2048]{1,0:T(8,128)(2,1)S(1)}, bf16[32,2048]{1,0:T(8,128)(2,1)S(1)}, u32[]{:S(2)}, u32[]{:S(2)}) collective-permute-start(bf16[32,2048]{1,0:T(8,128)(2,1)S(1)} %fusion.6), channel_id=1, source_target_pairs={{0,2},{1,3},{2,0},{3,1},{4,6},{5,7},{6,4},{7,5},{8,10},{9,11},{10,... | collective-permute-start | bytes 393224 | tf_op jit(solution)/shard_map/ppermute | solution.py:307
  51.4 9.7 %collective-permute-start.21 = (bf16[32,2048]{1,0:T(8,128)(2,1)S(1)}, bf16[32,2048]{1,0:T(8,128)(2,1)S(1)}, u32[]{:S(2)}, u32[]{:S(2)}) collective-permute-start(bf16[32,2048]{1,0:T(8,128)(2,1)S(1)} %fusion.3), channel_id=1, source_target_pairs={{0,2},{1,3},{2,0},{3,1},{4,6},{5,7},{6,4},{7,5},{8,10},{9,11},{10,... | collective-permute-start | bytes 393224 | tf_op jit(solution)/shard_map/ppermute | solution.py:307
  53.2 10.2 %collective-permute-start.28 = (bf16[32,2048]{1,0:T(8,128)(2,1)S(1)}, bf16[32,2048]{1,0:T(8,128)(2,1)S(1)}, u32[]{:S(2)}, u32[]{:S(2)}) collective-permute-start(bf16[32,2048]{1,0:T(8,128)(2,1)S(1)} %fusion), channel_id=1, source_target_pairs={{0,2},{1,3},{2,0},{3,1},{4,6},{5,7},{6,4},{7,5},{8,10},{9,11},{10,... | collective-permute-start | bytes 393224 | tf_op jit(solution)/shard_map/ppermute | solution.py:307
  58.4 7.3 %collective-permute-start.15 = (bf16[32,2048]{1,0:T(8,128)(2,1)S(1)}, bf16[32,2048]{1,0:T(8,128)(2,1)S(1)}, u32[]{:S(2)}, u32[]{:S(2)}) collective-permute-start(bf16[32,2048]{1,0:T(8,128)(2,1)S(1)} %fusion.8), channel_id=1, source_target_pairs={{0,4},{4,0},{8,12},{12,8},{1,5},{5,1},{9,13},{13,9},{2,6},{6,2},{1... | collective-permute-start | bytes 393224 | tf_op jit(solution)/shard_map/ppermute | solution.py:312
  61.2 11.3 %collective-permute-start.22 = (bf16[32,2048]{1,0:T(8,128)(2,1)S(1)}, bf16[32,2048]{1,0:T(8,128)(2,1)S(1)}, u32[]{:S(2)}, u32[]{:S(2)}) collective-permute-start(bf16[32,2048]{1,0:T(8,128)(2,1)S(1)} %fusion.5), channel_id=1, source_target_pairs={{0,8},{4,12},{8,0},{12,4},{1,9},{5,13},{9,1},{13,5},{2,10},{6,14},... | collective-permute-start | bytes 393224 | tf_op jit(solution)/shard_map/ppermute | solution.py:312
  63.5 9.0 %collective-permute-start.29 = (bf16[32,2048]{1,0:T(8,128)(2,1)S(1)}, bf16[32,2048]{1,0:T(8,128)(2,1)S(1)}, u32[]{:S(2)}, u32[]{:S(2)}) collective-permute-start(bf16[32,2048]{1,0:T(8,128)(2,1)S(1)} %fusion.2), channel_id=1, source_target_pairs={{0,12},{4,8},{8,4},{12,0},{1,13},{5,9},{9,5},{13,1},{2,14},{6,10},... | collective-permute-start | bytes 393224 | tf_op jit(solution)/shard_map/ppermute | solution.py:312
  (6 other events, 21.4 us)
